TPU v7x, 256 devices: a 8x8x2 block of a 8x8x16 slice. The times are simulated.
256 devices in a mesh: grp: 2 (over z), ep: 64 (over y, x), tp: 2 (over core).
Axes of the slice: x: 8, y: 8, z: 2, core: 2. Of those that a mesh axis runs over, the one named last changes fastest.
The devices are a block of a 8x8x16 slice.
Arguments:
- tokens_in: bfloat16 [8192, 2048], P(('grp', 'ep')), parts along dimension 0, may hold values from -6 to 6
- norm_gain: float32 [2048], replicated, may hold values from 0.1 to 1.9
- gate_proj: bfloat16 [64, 2048, 1024], P('ep', None, 'tp'), may hold values from -0.125 to 0.125
- up_proj: bfloat16 [64, 2048, 1024], P('ep', None, 'tp'), may hold values from -0.125 to 0.125
- down_proj: bfloat16 [64, 1024, 2048], P('ep', 'tp'), may hold values from -0.1875 to 0.1875
- route_ids: int32 [8192, 8], P(('grp', 'ep')), parts along dimension 0, may hold values from 0 to 63, all different within a row; in each aligned block of 64 rows (0 to 63, 64 to 127, ...) at most 16 rows name the same one
- group_weight: float32 [8192, 8], P(('grp', 'ep')), parts along dimension 0, may hold values from 0.05 to 1
- expert_weight: float32 [8192, 8], P(('grp', 'ep')), parts along dimension 0, may hold values from 0.05 to 1
Outputs:
- expert_mix: bfloat16 [8192, 2048], P(('grp', 'ep'), 'tp'), parts along dimension 0
There are 2 independent parts, one for each index of `grp`. A program takes and returns all parts, laid end to end along the dimension named above; an argument that names none is the same for every part. Nothing has to cross between parts.
Inputs may be any that keep to these rules, and one draw needn't show every extreme that they name: `route_ids`: each row names 8 different experts; within the rows of one index of ep no expert is named by more than 16 rows, a bound that some of them reach.
All inputs are finite; a program needn't handle non-finite values.
Results may differ from a plain program's by a relative error of at most 0.0077.
Values may be sent and summed in bfloat16 or wider, within the bound.
A program may use at most 64 MiB of HBM per device.

v0:
```python
import jax
import jax.numpy as jnp
from jax import lax
from jax.sharding import PartitionSpec as P

TOP = 8
EXP_GRP = 8
EPSILON = 1e-06


def cut_along(array, dim, size):
    lengths = array.shape
    blocks = array.reshape(*lengths[:dim], size, lengths[dim] // size, *lengths[dim + 1 :])
    return jnp.moveaxis(blocks, dim, 0)


def sum_at_owner(array, axis, dim):
    size = lax.axis_size(axis)
    blocks = lax.all_to_all(cut_along(array, dim, size), axis, 0, 0, tiled=True)
    return jnp.sum(blocks.astype(jnp.float32), axis=0)


def on_device(
    tokens_in, norm_gain, gate_proj, up_proj, down_proj, route_ids, group_weight, expert_weight
):
    token_count, model_width = tokens_in.shape
    expert_count = gate_proj.shape[0] * lax.axis_size("ep")
    lane_count = lax.axis_size("tp")
    part_width = model_width // lane_count
    capacity = min(token_count, max(2, 2 * token_count * TOP // expert_count))
    slot_total = expert_count * capacity
    row_values = tokens_in.astype(jnp.float32)
    inv_scale = lax.rsqrt(jnp.mean(row_values * row_values, axis=-1, keepdims=True) + EPSILON)
    normed = (row_values * inv_scale * norm_gain).astype(jnp.bfloat16)
    route_count = token_count * TOP
    flat_ids = route_ids.reshape(route_count)
    positions = jnp.arange(route_count, dtype=jnp.int32)
    same_expert = (flat_ids[:, None] == flat_ids[None, :]) & (
        positions[None, :] < positions[:, None]
    )
    slot_rank = jnp.sum(same_expert.astype(jnp.int32), axis=1)
    slot_index = flat_ids * capacity + slot_rank
    slot_match = jnp.arange(slot_total, dtype=jnp.int32)[:, None] == slot_index[None, :]
    selector = jnp.sum(
        slot_match.reshape(slot_total, token_count, TOP).astype(jnp.int32), axis=2
    ).astype(jnp.bfloat16)
    gate_local = gate_proj[0]
    up_local = up_proj[0]
    lane_index = lax.axis_index("tp")
    own_half = lax.dynamic_slice_in_dim(normed, lane_index * part_width, part_width, 1)
    outgoing = jnp.dot(selector, own_half, preferred_element_type=jnp.float32).astype(jnp.bfloat16)
    arrived = lax.all_to_all(
        outgoing.reshape(expert_count, capacity, part_width),
        "ep",
        split_axis=0,
        concat_axis=0,
        tiled=True,
    )
    arrived = arrived.reshape(slot_total, part_width)
    column_piece = lax.all_gather(arrived, "tp", axis=1, tiled=True)
    gate_acts = jnp.dot(column_piece, gate_local, preferred_element_type=jnp.float32)
    up_acts = jnp.dot(column_piece, up_local, preferred_element_type=jnp.float32)
    hidden = (jax.nn.silu(gate_acts) * up_acts).astype(jnp.bfloat16)
    partial_rows = jnp.dot(hidden, down_proj[0], preferred_element_type=jnp.float32)
    summed = sum_at_owner(
        partial_rows.reshape(expert_count, capacity, model_width).astype(jnp.bfloat16), "tp", 2
    )
    results = summed.astype(jnp.bfloat16)
    returned = lax.all_to_all(results, "ep", split_axis=0, concat_axis=0, tiled=True).reshape(
        slot_total, part_width
    )
    picked = returned[slot_index].astype(jnp.float32).reshape(token_count, TOP, part_width)
    group_ids = route_ids // EXP_GRP
    group_count = group_weight.shape[1]
    group_match = (
        group_ids[:, :, None] == jnp.arange(group_count, dtype=jnp.int32)[None, None, :]
    ).astype(jnp.float32)
    group_part = jnp.sum(group_weight[:, None, :] * group_match, axis=2)
    gate_values = group_part * expert_weight / jnp.sum(expert_weight, axis=1, keepdims=True)
    return jnp.sum(picked * gate_values[:, :, None], axis=1).astype(jnp.bfloat16)


def solution(mesh):
    in_specs = (
        P(("grp", "ep"), None),
        P(),
        P("ep", None, "tp"),
        P("ep", None, "tp"),
        P("ep", "tp", None),
        P(("grp", "ep"), None),
        P(("grp", "ep"), None),
        P(("grp", "ep"), None),
    )
    out_specs = P(("grp", "ep"), "tp")
    return jax.shard_map(
        on_device, mesh=mesh, in_specs=in_specs, out_specs=out_specs, check_vma=False
    )
```

profile of v0, /device:TPU:514, one launch (start us, length us, event | category | flops | bytes accessed | tf_op | source)
XLA Modules:
  0.0 216.0 jit_solution(7506265072580166607)
XLA Ops:
  6.6 1.1 convert_element_type.40
  7.7 1.1 multiply_reduce_fusion
  8.8 0.8 copy.24
  9.6 0.1 eq.43
  9.7 0.3 convert_reduce_fusion.1
  9.9 0.1 reduce_sum.71
  10.0 0.7 convert_reduce_fusion
  10.7 0.7 dynamic-slice
  11.4 0.8 convolution_convert_fusion.1
  12.2 72.0 %all_to_all.15 = bf16[64,16,1024]{2,1,0:T(8,128)(2,1)} all-to-all(bf16[64,16,1024]{2,1,0:T(8,128)(2,1)S(1)} %bitcast.33), channel_id=1, replica_groups=mesh['grp'=2,'ep'=64,'tp'=2] {'ep'}, dimensions={0} | all-to-all | bytes 4194304 | tf_op jit(solution)/shard_map/all_to_all | solution.py:52
  84.2 0.1 all-gather.2.cloned.1.call-update
  84.2 28.4 %all-gather.2.cloned.1.call-done = bf16[1024,2048]{1,0:T(8,128)(2,1)} async-done(((bf16[1024,1024]{1,0:T(8,128)(2,1)}), bf16[1024,2048]{1,0:T(8,128)(2,1)}) %all-gather.2.cloned.1.call-update) | async-done | bytes 4194320 | tf_op jit(solution)/shard_map/all_gather | solution.py:60
  112.7 5.3 %fusion.2 = f32[1024,512]{1,0:T(8,128)S(1)} fusion(bf16[1024,2048]{1,0:T(8,128)(2,1)} %all-gather.2.cloned.1.call-done, bf16[1,2048,512]{2,1,0:T(8,128)(2,1)} %param.11), kind=kOutput, calls=%fused_computation.6 | convolution fusion | flops 2147483648 | bytes 8388608 | tf_op jit(solution)/shard_map/dot_general | solution.py:62
  118.0 2.6 %multiply_convert_fusion = bf16[1024,512]{1,0:T(8,128)(2,1)S(1)} fusion(f32[1024,512]{1,0:T(8,128)S(1)} %fusion.2, bf16[1024,2048]{1,0:T(8,128)(2,1)S(1)} %copy-done.4, bf16[1,2048,512]{2,1,0:T(8,128)(2,1)S(1)} %copy-done.5), kind=kOutput, calls=%fused_computation.10 | convolution fusion | flops 2150629376 | bytes 9437184 | tf_op jit(solution)/shard_map/dot_general | solution.py:61
  120.7 2.3 %convolution_convert_fusion = bf16[64,16,2048]{2,1,0:T(8,128)(2,1)S(1)} fusion(bf16[64,16,512]{2,1,0:T(8,128)(2,1)S(1)} %bitcast.37, bf16[1,512,2048]{2,1,0:T(8,128)(2,1)S(1)} %copy-done), kind=kOutput, calls=%fused_computation.2 | convolution fusion | flops 2149580800 | bytes 7340032 | tf_op jit(solution)/shard_map/dot_general | solution.py:64
  123.0 0.6 copy.30
  123.7 8.2 %all_to_all.16 = bf16[2,64,16,1024]{3,2,1,0:T(8,128)(2,1)} all-to-all(bf16[2,64,16,1024]{3,2,1,0:T(8,128)(2,1)S(1)} %bitcast.31), channel_id=1, replica_groups=mesh['grp'=2,'ep'=64,'tp'=2] {'tp'}, dimensions={0} | all-to-all | bytes 8388608 | tf_op jit(solution)/shard_map/all_to_all | solution.py:19
  131.8 5.2 %reduce_sum.74 = bf16[64,16,1024]{2,1,0:T(8,128)(2,1)} reduce(bf16[2,64,16,1024]{3,2,1,0:T(8,128)(2,1)} %all_to_all.16, bf16[]{:T(256)} %constant.37.clone.1), dimensions={0}, to_apply=%region_3.4 | reduce | flops 1048576 | bytes 6291458 | tf_op jit(solution)/shard_map/reduce_sum | solution.py:20
  137.1 13.9 %all-to-all-start.2 = ((bf16[64,16,1024]{2,1,0:T(8,128)(2,1)}), bf16[64,16,1024]{2,1,0:T(8,128)(2,1)}, u32[]{:S(2)}, u32[]{:S(2)}) async-start(bf16[64,16,1024]{2,1,0:T(8,128)(2,1)} %reduce_sum.74), calls=%async_computation.2 | async-start | bytes 4194304 | tf_op jit(solution)/shard_map/all_to_all | solution.py:69
  150.9 0.1 mul.78
  151.1 0.1 copy.27
  151.2 51.9 %all-to-all-done.2 = bf16[64,16,1024]{2,1,0:T(8,128)(2,1)} async-done(((bf16[64,16,1024]{2,1,0:T(8,128)(2,1)}), bf16[64,16,1024]{2,1,0:T(8,128)(2,1)}, u32[]{:S(2)}, u32[]{:S(2)}) %all-to-all-start.2) | async-done | bytes 2097184 | tf_op jit(solution)/shard_map/all_to_all | solution.py:69
  203.2 4.6 %gather_fusion = bf16[512,1024]{1,0:T(8,128)(2,1)S(1)} fusion(bf16[1024,1024]{1,0:T(8,128)(2,1)} %bitcast.8, s32[1024]{0:T(1024)S(1)} %pad_clamp_fusion), kind=kCustom, calls=%fused_computation | custom fusion | bytes 2099200 | tf_op jit(solution)/shard_map/gather | solution.py:72
  207.8 1.4 fusion
  (21 shorter events, 0.1 us)
Async XLA Ops:
  6.5 114.1 %copy-start = (bf16[1,512,2048]{2,1,0:T(8,128)(2,1)S(1)}, bf16[1,512,2048]{2,1,0:T(8,128)(2,1)}, u32[]{:S(2)}) copy-start(bf16[1,512,2048]{2,1,0:T(8,128)(2,1)} %param.12) | copy-start | bytes 6291460
  6.6 106.1 %all-gather.2.cloned.1.call-start = ((), (), s32[]{:S(2)}) async-start(), calls=%async_computation.3 | async-start | bytes 6291456 | tf_op jit(solution)/shard_map/all_gather | solution.py:60
  112.6 5.3 %copy-start.4 = (bf16[1024,2048]{1,0:T(8,128)(2,1)S(1)}, bf16[1024,2048]{1,0:T(8,128)(2,1)}, u32[]{:S(2)}) copy-start(bf16[1024,2048]{1,0:T(8,128)(2,1)} %all-gather.2.cloned.1.call-done) | copy-start | bytes 12582916
  112.6 5.3 %copy-start.5 = (bf16[1,2048,512]{2,1,0:T(8,128)(2,1)S(1)}, bf16[1,2048,512]{2,1,0:T(8,128)(2,1)}, u32[]{:S(2)}) copy-start(bf16[1,2048,512]{2,1,0:T(8,128)(2,1)} %param.10) | copy-start | bytes 6291460
  137.1 14.0 %copy-start.1 = (f32[64,8]{0,1:T(8,128)S(1)}, f32[64,8]{0,1:T(8,128)}, u32[]{:S(2)}) copy-start(f32[64,8]{0,1:T(8,128)} %param.15) | copy-start | bytes 6148
  137.1 14.0 %copy-start.2 = (s32[64,8]{0,1:T(8,128)S(1)}, s32[64,8]{0,1:T(8,128)}, u32[]{:S(2)}) copy-start(s32[64,8]{0,1:T(8,128)} %param.13) | copy-start | bytes 6148
  137.1 14.0 %copy-start.3 = (f32[64,8]{0,1:T(8,128)S(1)}, f32[64,8]{0,1:T(8,128)}, u32[]{:S(2)}) copy-start(f32[64,8]{0,1:T(8,128)} %param.14) | copy-start | bytes 6148
  137.1 66.1 %all-to-all-start.2 = ((bf16[64,16,1024]{2,1,0:T(8,128)(2,1)}), bf16[64,16,1024]{2,1,0:T(8,128)(2,1)}, u32[]{:S(2)}, u32[]{:S(2)}) async-start(bf16[64,16,1024]{2,1,0:T(8,128)(2,1)} %reduce_sum.74), calls=%async_computation.2 | async-start | bytes 4194304 | tf_op jit(solution)/shard_map/all_to_all | solution.py:69
Sparse Core Ops, SparseCore 0:
  84.4 28.2 all-gather.1
where the time goes:
time: 216 us
  waiting for transfers between devices  80.4 us (37%)
  blocking collectives  80.2 us (37%)
  starting transfers between devices  13.9 us (6%)
  between operations  13.6 us (6%)
  matrix products  11.1 us (5%)
  other arithmetic  9.82 us (5%)
  local copies, waits for them, and re-layouts  7.08 us (3%)
    all_to_all x1, blocking collectives, on_device(): lax.all_to_all(outgoing.reshape(expert_count, capacity, part_width), 'ep'...  72 us
    all_to_all x1, waiting for transfers between devices, on_device(): lax.all_to_all(results, 'ep', split_axis=0, concat_axis=0, tiled=True)  51.9 us
    all_gather x1, waiting for transfers between devices, on_device(): column_piece = lax.all_gather(arrived, 'tp', axis=1, tiled=True)  28.4 us
    all_to_all x1, starting transfers between devices, on_device(): lax.all_to_all(results, 'ep', split_axis=0, concat_axis=0, tiled=True)  13.9 us
    all_to_all x1, blocking collectives, sum_at_owner(): blocks = lax.all_to_all(cut_along(array, dim, size), axis, 0, 0, tiled=True)  8.19 us
    dot_general x1, matrix products, on_device(): jnp.dot(column_piece, up_local, preferred_element_type=jnp.float32)  5.32 us
    reduce_sum x1, other arithmetic, sum_at_owner(): return jnp.sum(blocks.astype(jnp.float32), axis=0)  5.22 us
    gather x1, local copies, waits for them, and re-layouts, on_device(): returned[slot_index].astype(jnp.float32)  4.59 us
  transfers between devices with their start and end apart: 2, of which 2 were waited for; matrix products, arithmetic and copies ran while one was open for 0% of the time, Pallas kernels for 0%

commit v1 on v0

--- a/solution.py
+++ b/solution.py
@@ -57,7 +57,8 @@
         tiled=True,
     )
     arrived = arrived.reshape(slot_total, part_width)
-    column_piece = lax.all_gather(arrived, "tp", axis=1, tiled=True)
+    copies = jnp.concatenate([arrived] * lax.axis_size("tp"), axis=1)
+    column_piece = lax.all_to_all(copies, "tp", 1, 1, tiled=True)
     gate_acts = jnp.dot(column_piece, gate_local, preferred_element_type=jnp.float32)
     up_acts = jnp.dot(column_piece, up_local, preferred_element_type=jnp.float32)
     hidden = (jax.nn.silu(gate_acts) * up_acts).astype(jnp.bfloat16)

time: 216 us -> 187 us (0.87); the launches traced: 216 us -> 183 us
  waiting for transfers between devices: 80.4 us -> 52 us
  between operations: 13.6 us -> 0.18 us
  blocking collectives: 80.2 us -> 88.1 us
  local copies, waits for them, and re-layouts: 7.08 us -> 13.3 us
  starting transfers between devices: 13.9 us -> 8.42 us
    all_gather x1 -> x0, waiting for transfers between devices: 28.4 us -> none  [on_device(): column_piece = lax.all_gather(arrived, 'tp', axis=1, tiled=True)]
    all_to_all x0 -> x1, blocking collectives: none -> 8.19 us  [on_device(): column_piece = lax.all_to_all(copies, 'tp', 1, 1, tiled=True)]
    all_to_all x0 -> x1, local copies, waits for them, and re-layouts: none -> 6.21 us  [on_device(): column_piece = lax.all_to_all(copies, 'tp', 1, 1, tiled=True)]
    all_to_all x1, starting transfers between devices: 13.9 us -> 8.42 us  [on_device(): lax.all_to_all(results, 'ep', split_axis=0, concat_axis=0, tiled=True)]
  transfers between devices with their start and end apart: 2 -> 1, of which waited for: 2 -> 1; matrix products, arithmetic and copies ran while one was open for 0% -> 0% of each run, Pallas kernels for 0% -> 0%
where the time goes in v1:
time: 187 us; the launch traced here: 183 us
  blocking collectives  88.1 us (47%)
  waiting for transfers between devices  52 us (28%)
  local copies, waits for them, and re-layouts  13.3 us (7%)
  matrix products  11.2 us (6%)
  other arithmetic  10.2 us (5%)
  starting transfers between devices  8.42 us (5%)
    all_to_all x1, blocking collectives, on_device(): lax.all_to_all(outgoing.reshape(expert_count, capacity, part_width), 'ep'...  71.8 us
    all_to_all x1, waiting for transfers between devices, on_device(): lax.all_to_all(results, 'ep', split_axis=0, concat_axis=0, tiled=True)  52 us
    all_to_all x1, starting transfers between devices, on_device(): lax.all_to_all(results, 'ep', split_axis=0, concat_axis=0, tiled=True)  8.42 us
    all_to_all x1, blocking collectives, sum_at_owner(): blocks = lax.all_to_all(cut_along(array, dim, size), axis, 0, 0, tiled=True)  8.19 us
    all_to_all x1, blocking collectives, on_device(): column_piece = lax.all_to_all(copies, 'tp', 1, 1, tiled=True)  8.19 us
    all_to_all x1, local copies, waits for them, and re-layouts, on_device(): column_piece = lax.all_to_all(copies, 'tp', 1, 1, tiled=True)  6.21 us
    dot_general x1, matrix products, on_device(): jnp.dot(column_piece, up_local, preferred_element_type=jnp.float32)  5.36 us
    reduce_sum x1, other arithmetic, sum_at_owner(): return jnp.sum(blocks.astype(jnp.float32), axis=0)  5.22 us
  transfers between devices with their start and end apart: 1, of which 1 were waited for; matrix products, arithmetic and copies ran while one was open for 0% of the time, Pallas kernels for 0%

profile of v1, /device:TPU:514, one launch (start us, length us, event | category | flops | bytes accessed | tf_op | source)
XLA Modules:
  0.0 183.4 jit_solution(10522812720829425600)
XLA Ops:
  0.0 1.1 convert_element_type.40
  1.1 1.1 multiply_reduce_fusion
  2.3 0.8 copy.32
  3.0 0.1 eq.43
  3.1 0.3 convert_reduce_fusion.1
  3.4 0.1 reduce_sum.71
  3.5 0.7 convert_reduce_fusion
  4.2 0.7 dynamic-slice
  4.9 0.8 convolution_convert_fusion.1
  5.6 71.8 %all_to_all.24 = bf16[64,16,1024]{2,1,0:T(8,128)(2,1)S(1)} all-to-all(bf16[64,16,1024]{2,1,0:T(8,128)(2,1)S(1)} %bitcast.36), channel_id=1, replica_groups=mesh['grp'=2,'ep'=64,'tp'=2] {'ep'}, dimensions={0} | all-to-all | bytes 4194304 | tf_op jit(solution)/shard_map/all_to_all | solution.py:52
  77.4 0.4 pad_maximum_fusion
  77.8 8.2 %all_to_all.25 = bf16[1024,2,1024]{2,0,1:T(8,128)(2,1)} all-to-all(bf16[1024,2,1024]{2,0,1:T(8,128)(2,1)S(1)} %pad_maximum_fusion), channel_id=1, replica_groups=mesh['grp'=2,'ep'=64,'tp'=2] {'tp'}, dimensions={1} | all-to-all | bytes 8388608 | tf_op jit(solution)/shard_map/all_to_all | solution.py:61
  86.0 6.2 %copy.34 = bf16[1024,2,1024]{0,2,1:T(8,128)(2,1)} copy(bf16[1024,2,1024]{2,0,1:T(8,128)(2,1)} %all_to_all.25) | data formatting | bytes 8388608 | tf_op jit(solution)/shard_map/all_to_all | solution.py:61
  92.2 5.4 %fusion.2 = f32[1024,512]{1,0:T(8,128)S(1)} fusion(bf16[1024,2048]{0,1:T(8,128)(2,1)} %bitcast.32, bf16[1,2048,512]{2,1,0:T(8,128)(2,1)} %param.11), kind=kOutput, calls=%fused_computation.7 | convolution fusion | flops 2147483648 | bytes 8388608 | tf_op jit(solution)/shard_map/dot_general | solution.py:63
  97.6 2.7 %multiply_convert_fusion = bf16[1024,512]{1,0:T(8,128)(2,1)S(1)} fusion(f32[1024,512]{1,0:T(8,128)S(1)} %fusion.2, bf16[1024,2048]{0,1:T(8,128)(2,1)S(1)} %bitcast.33, bf16[1,2048,512]{2,1,0:T(8,128)(2,1)S(1)} %copy-done.5), kind=kOutput, calls=%fused_computation.11 | convolution fusion | flops 2150629376 | bytes 9437184 | tf_op jit(solution)/shard_map/dot_general | solution.py:62
  100.3 2.4 %convolution_convert_fusion = bf16[64,16,2048]{2,1,0:T(8,128)(2,1)S(1)} fusion(bf16[64,16,512]{2,1,0:T(8,128)(2,1)S(1)} %bitcast.40, bf16[1,512,2048]{2,1,0:T(8,128)(2,1)S(1)} %copy-done), kind=kOutput, calls=%fused_computation.3 | convolution fusion | flops 2149580800 | bytes 7340032 | tf_op jit(solution)/shard_map/dot_general | solution.py:65
  102.7 0.6 copy.39
  103.3 8.2 %all_to_all.26 = bf16[2,64,16,1024]{3,2,1,0:T(8,128)(2,1)} all-to-all(bf16[2,64,16,1024]{3,2,1,0:T(8,128)(2,1)S(1)} %bitcast.34), channel_id=1, replica_groups=mesh['grp'=2,'ep'=64,'tp'=2] {'tp'}, dimensions={0} | all-to-all | bytes 8388608 | tf_op jit(solution)/shard_map/all_to_all | solution.py:19
  111.5 5.2 %reduce_sum.74 = bf16[64,16,1024]{2,1,0:T(8,128)(2,1)} reduce(bf16[2,64,16,1024]{3,2,1,0:T(8,128)(2,1)} %all_to_all.26, bf16[]{:T(256)} %constant.37.clone.1), dimensions={0}, to_apply=%region_3.4 | reduce | flops 1048576 | bytes 6291458 | tf_op jit(solution)/shard_map/reduce_sum | solution.py:20
  116.7 8.4 %all-to-all-start.3 = ((bf16[64,16,1024]{2,1,0:T(8,128)(2,1)}), bf16[64,16,1024]{2,1,0:T(8,128)(2,1)}, u32[]{:S(2)}, u32[]{:S(2)}) async-start(bf16[64,16,1024]{2,1,0:T(8,128)(2,1)} %reduce_sum.74), calls=%async_computation.3 | async-start | bytes 4194304 | tf_op jit(solution)/shard_map/all_to_all | solution.py:70
  125.2 0.1 mul.78
  125.4 52.0 %all-to-all-done.3 = bf16[64,16,1024]{2,1,0:T(8,128)(2,1)} async-done(((bf16[64,16,1024]{2,1,0:T(8,128)(2,1)}), bf16[64,16,1024]{2,1,0:T(8,128)(2,1)}, u32[]{:S(2)}, u32[]{:S(2)}) %all-to-all-start.3) | async-done | bytes 2097184 | tf_op jit(solution)/shard_map/all_to_all | solution.py:70
  177.5 4.6 %gather_fusion = bf16[512,1024]{1,0:T(8,128)(2,1)S(1)} fusion(bf16[1024,1024]{1,0:T(8,128)(2,1)} %bitcast.9, s32[1024]{0:T(1024)S(1)} %pad_clamp_fusion), kind=kCustom, calls=%fused_computation | custom fusion | bytes 2099200 | tf_op jit(solution)/shard_map/gather | solution.py:73
  182.1 1.3 fusion
  (21 shorter events, 0.2 us)
Async XLA Ops:
  0.0 100.3 %copy-start = (bf16[1,512,2048]{2,1,0:T(8,128)(2,1)S(1)}, bf16[1,512,2048]{2,1,0:T(8,128)(2,1)}, u32[]{:S(2)}) copy-start(bf16[1,512,2048]{2,1,0:T(8,128)(2,1)} %param.12) | copy-start | bytes 6291460
  92.2 5.4 %copy-start.1 = (bf16[1024,2,1024]{0,2,1:T(8,128)(2,1)S(1)}, bf16[1024,2,1024]{0,2,1:T(8,128)(2,1)}, u32[]{:S(2)}) copy-start(bf16[1024,2,1024]{0,2,1:T(8,128)(2,1)} %copy.34) | copy-start | bytes 12582916
  92.2 5.4 %copy-start.5 = (bf16[1,2048,512]{2,1,0:T(8,128)(2,1)S(1)}, bf16[1,2048,512]{2,1,0:T(8,128)(2,1)}, u32[]{:S(2)}) copy-start(bf16[1,2048,512]{2,1,0:T(8,128)(2,1)} %param.10) | copy-start | bytes 6291460
  116.7 8.5 %copy-start.2 = (f32[64,8]{0,1:T(8,128)S(1)}, f32[64,8]{0,1:T(8,128)}, u32[]{:S(2)}) copy-start(f32[64,8]{0,1:T(8,128)} %param.15) | copy-start | bytes 6148
  116.7 8.6 %copy-start.3 = (s32[64,8]{0,1:T(8,128)S(1)}, s32[64,8]{0,1:T(8,128)}, u32[]{:S(2)}) copy-start(s32[64,8]{0,1:T(8,128)} %param.13) | copy-start | bytes 6148
  116.7 8.6 %copy-start.4 = (f32[64,8]{0,1:T(8,128)S(1)}, f32[64,8]{0,1:T(8,128)}, u32[]{:S(2)}) copy-start(f32[64,8]{0,1:T(8,128)} %param.14) | copy-start | bytes 6148
  116.7 60.8 %all-to-all-start.3 = ((bf16[64,16,1024]{2,1,0:T(8,128)(2,1)}), bf16[64,16,1024]{2,1,0:T(8,128)(2,1)}, u32[]{:S(2)}, u32[]{:S(2)}) async-start(bf16[64,16,1024]{2,1,0:T(8,128)(2,1)} %reduce_sum.74), calls=%async_computation.3 | async-start | bytes 4194304 | tf_op jit(solution)/shard_map/all_to_all | solution.py:70
